TPU v7x, 32 devices: a whole 2x2x4 slice. The times are simulated.
32 devices in a mesh: grp: 2 (over y), ep: 4 (over z), tp: 4 (over x, core).
Axes of the slice: x: 2, y: 2, z: 4, core: 2. Of those that a mesh axis runs over, the one named last changes fastest.
Arguments:
- queries: bfloat16 [2048, 2048], P(('grp', 'ep'), 'tp'), parts along dimension 0, may hold values from -8 to 8
- keys: bfloat16 [2048, 512], P(('grp', 'ep')), parts along dimension 0, may hold values from -8 to 8
- values: bfloat16 [2048, 512], P(('grp', 'ep')), parts along dimension 0, may hold values from -6 to 6
- q_gain: float32 [128], replicated, may hold values from 0.6 to 5.8
- k_gain: float32 [128], replicated, may hold values from 0.6 to 5.8
- w_out: bfloat16 [2048, 2048], P(None, 'tp'), may hold values from -0.125 to 0.125
- moe_rows: bfloat16 [1536, 2048], P(('grp', 'ep')), parts along dimension 0, may hold values from -6 to 6
- routes: int32 [1536, 2], P(('grp', 'ep')), parts along dimension 0, may hold values from 0 to 3, all different within a row; in each aligned block of 192 rows (0 to 191, 192 to 383, ...) at most 144 rows name the same one
- group_gate: float32 [1536], P(('grp', 'ep')), parts along dimension 0, may hold values from 0.25 to 1
- expert_logits: float32 [1536, 2], P(('grp', 'ep')), parts along dimension 0, may hold values from -6 to 6
- moe_gain: float32 [2048], replicated, may hold values from 0.1 to 1.9
- w_gate: bfloat16 [4, 2048, 2048], P('ep', None, 'tp'), may hold values from -0.125 to 0.125
- w_up: bfloat16 [4, 2048, 2048], P('ep', None, 'tp'), may hold values from -0.125 to 0.125
- w_down: bfloat16 [4, 2048, 2048], P('ep', 'tp'), may hold values from -0.125 to 0.125
Outputs:
- attn_out: bfloat16 [2048, 2048], P(('grp', 'ep'), 'tp'), parts along dimension 0
- moe_out: bfloat16 [1536, 2048], P(('grp', 'ep'), 'tp'), parts along dimension 0
There are 2 independent parts, one for each index of `grp`. A program takes and returns all parts, laid end to end along the dimension named above; an argument that names none is the same for every part. Nothing has to cross between parts.
Inputs may be any that keep to these rules, and one draw needn't show every extreme that they name: `routes`: each row names 2 different experts; within the rows of one index of ep no expert is named more than 144 times, a bound that some block reaches.
All inputs are finite; a program needn't handle non-finite values.
Results may differ from a plain program's by a relative error of at most 0.019.
The roundings to bfloat16 on the way count: a program that leaves them out, or rounds other values in their place, can miss the bound.
Values may be sent and summed in bfloat16 or wider, within the bound.
A program may use at most 64 MiB of HBM per device.

v0:
```python
import jax
import jax.numpy as jnp
from jax import lax
from jax.sharding import PartitionSpec as P

HEADS = 16
KV_HEADS = 4
HEAD_DIM = 128
GRID_W = 64
TOPK = 2


def head_norm(x, gain):
    wide = x.astype(jnp.float32)
    return wide * lax.rsqrt(jnp.mean(wide * wide, axis=-1, keepdims=True) + 1e-06) * gain


def rotate(x, first):
    count = x.shape[0]
    pos = first + jnp.arange(count, dtype=jnp.int32)
    row = (pos // GRID_W).astype(jnp.float32)
    col = (pos % GRID_W).astype(jnp.float32)
    nfreq = HEAD_DIM // 4
    inverse = 10000.0 ** (-jnp.arange(nfreq, dtype=jnp.float32) / nfreq)
    angle = jnp.concatenate(
        [
            row[:, None] * inverse,
            row[:, None] * inverse,
            col[:, None] * inverse,
            col[:, None] * inverse,
        ],
        axis=1,
    )
    parts = x.reshape(x.shape[:-1] + (2, 2, nfreq))
    turned = jnp.stack([-parts[..., 1, :], parts[..., 0, :]], axis=-2).reshape(x.shape)
    return x * jnp.cos(angle)[:, None, :] + turned * jnp.sin(angle)[:, None, :]


def per_device(
    queries,
    keys,
    values,
    q_gain,
    k_gain,
    w_out,
    moe_rows,
    routes,
    group_gate,
    expert_logits,
    moe_gain,
    w_gate,
    w_up,
    w_down,
):
    rows = queries.shape[0]
    heads_dev = queries.shape[1] // HEAD_DIM
    group = HEADS // KV_HEADS
    kv_dev = max(1, heads_dev // group)
    per_kv = heads_dev // kv_dev
    first_kv = lax.axis_index("tp") * heads_dev // group
    first_row = lax.axis_index("ep") * rows
    k_mine = lax.dynamic_slice_in_dim(keys, first_kv * HEAD_DIM, kv_dev * HEAD_DIM, 1)
    v_mine = lax.dynamic_slice_in_dim(values, first_kv * HEAD_DIM, kv_dev * HEAD_DIM, 1)
    k_rot = rotate(head_norm(k_mine.reshape(rows, kv_dev, HEAD_DIM), k_gain), first_row)
    k_rot = k_rot.astype(jnp.bfloat16).reshape(rows, kv_dev * HEAD_DIM)
    q_rot = rotate(head_norm(queries.reshape(rows, heads_dev, HEAD_DIM), q_gain), first_row)
    q_rot = q_rot.astype(jnp.bfloat16).reshape(rows, kv_dev, per_kv, HEAD_DIM)
    scale = HEAD_DIM ** (-0.5)
    top = jnp.full((rows, kv_dev, per_kv), -jnp.inf, jnp.float32)
    total = jnp.zeros((rows, kv_dev, per_kv), jnp.float32)
    acc = jnp.zeros((rows, kv_dev, per_kv, HEAD_DIM), jnp.float32)
    k_piece = lax.all_gather(k_rot, "ep", axis=0, tiled=True)
    v_piece = lax.all_gather(v_mine, "ep", axis=0, tiled=True)
    count = k_piece.shape[0]
    key_rows = k_piece.reshape(count, kv_dev, HEAD_DIM)
    value_rows = v_piece.reshape(count, kv_dev, HEAD_DIM)
    scores = (
        jnp.einsum("qkgd,nkd->qkgn", q_rot, key_rows, preferred_element_type=jnp.float32) * scale
    )
    new_top = jnp.max(scores, axis=-1)
    shrink = jnp.exp(top - new_top)
    expo = jnp.exp(scores - new_top[..., None])
    total = total * shrink + jnp.sum(expo, axis=-1)
    acc = acc * shrink[..., None] + jnp.einsum(
        "qkgn,nkd->qkgd", expo.astype(jnp.bfloat16), value_rows, preferred_element_type=jnp.float32
    )
    top, total, acc = (new_top, total, acc)
    mixed = (acc / total[..., None]).astype(jnp.bfloat16).reshape(rows, heads_dev * HEAD_DIM)
    attn_out = jnp.dot(
        lax.all_gather(mixed, "tp", axis=1, tiled=True), w_out, preferred_element_type=jnp.float32
    ).astype(jnp.bfloat16)
    count = moe_rows.shape[0]
    width = moe_rows.shape[1]
    peers = lax.axis_size("ep")
    capacity = 3 * count // peers
    wide = moe_rows.astype(jnp.float32)
    normed = (
        wide * lax.rsqrt(jnp.mean(wide * wide, axis=-1, keepdims=True) + 1e-06) * moe_gain
    ).astype(jnp.bfloat16)
    chosen = routes.reshape(-1)
    onehot = (chosen[:, None] == jnp.arange(peers, dtype=jnp.int32)[None, :]).astype(jnp.int32)
    rank = jnp.sum((jnp.cumsum(onehot, axis=0) - onehot) * onehot, axis=1)
    slots = chosen * capacity + rank
    owner = jnp.arange(count * TOPK, dtype=jnp.int32) // TOPK
    source = jnp.zeros((peers * capacity,), jnp.int32).at[slots].set(owner)
    used = jnp.zeros((peers * capacity,), jnp.bool_).at[slots].set(True)
    outgoing = jnp.where(used[:, None], normed[source], jnp.zeros((), jnp.bfloat16)).reshape(
        peers, capacity, width
    )
    part_cols = width // lax.axis_size("tp")
    mine = lax.dynamic_slice_in_dim(outgoing, lax.axis_index("tp") * part_cols, part_cols, 2)
    arrived = lax.all_gather(
        lax.all_to_all(mine, "ep", split_axis=0, concat_axis=0, tiled=True),
        "tp",
        axis=2,
        tiled=True,
    )
    first_dim, second_dim, cols = arrived.shape
    flat = arrived.reshape(first_dim * second_dim, cols)
    gate = jnp.dot(flat, w_gate[0], preferred_element_type=jnp.float32)
    up = jnp.dot(flat, w_up[0], preferred_element_type=jnp.float32)
    hidden = (jax.nn.silu(gate) * up).astype(jnp.bfloat16)
    result = jnp.dot(hidden, w_down[0], preferred_element_type=jnp.float32).astype(jnp.bfloat16)
    partial_value = result.reshape(first_dim, second_dim, cols)
    summed = (
        lax.psum_scatter(partial_value, "tp", scatter_dimension=2, tiled=True)
        .astype(jnp.float32)
        .astype(jnp.bfloat16)
    )
    back = lax.all_to_all(summed, "ep", split_axis=0, concat_axis=0, tiled=True)
    back = back.reshape(peers * capacity, back.shape[2])
    picked = back[slots].astype(jnp.float32).reshape(count, TOPK, back.shape[1])
    weights = group_gate[:, None] * jax.nn.softmax(expert_logits, axis=-1)
    moe_out = jnp.sum(weights[:, :, None] * picked, axis=1).astype(jnp.bfloat16)
    return (attn_out, moe_out)


def solution(mesh):
    placed = (
        P(("grp", "ep"), "tp"),
        P(("grp", "ep"), None),
        P(("grp", "ep"), None),
        P(),
        P(),
        P(None, "tp"),
        P(("grp", "ep"), None),
        P(("grp", "ep"), None),
        P(("grp", "ep")),
        P(("grp", "ep"), None),
        P(),
        P("ep", None, "tp"),
        P("ep", None, "tp"),
        P("ep", "tp", None),
    )
    return jax.shard_map(
        per_device,
        mesh=mesh,
        in_specs=placed,
        out_specs=(P(("grp", "ep"), "tp"), P(("grp", "ep"), "tp")),
        check_vma=False,
    )
```

profile of v0, /device:TPU:0, one launch (start us, length us, event | category | flops | bytes accessed | tf_op | source)
XLA Modules:
  0.0 148.1 jit_solution(11262557061539180350)
XLA Ops:
  7.2 0.9 copy.30
  9.2 1.2 reduce-window.6
  11.2 2.9 %scatter_custom_fusion.1 = s32[576]{0:T(1024)S(1)} fusion(s32[384]{0:T(512)S(1)} %fusion.58, s32[384]{0:T(512)S(1)} %add_select_fusion, s32[]{:T(128)} %constant.95.clone.1), kind=kCustom, calls=%fused_computation.81 | custom fusion | bytes 2308 | tf_op jit(solution)/shard_map/scatter | solution.py:105
  14.1 1.4 fusion.13
  15.5 2.0 %scatter_custom_fusion = pred[576]{0:T(1024)(128)(4,1)S(1)} fusion(s32[384]{0:T(512)S(1)} %fusion.58, pred[384]{0:T(512)(128)(4,1)S(1)} %broadcast.278, pred[]{:T(512)} %constant.115.clone.1), kind=kCustom, calls=%fused_computation.86 | custom fusion | bytes 577 | tf_op jit(solution)/shard_map/scatter | solution.py:106
  17.6 1.4 fusion.15
  19.0 4.0 %gather_fusion = bf16[576,2048]{1,0:T(8,128)(2,1)} fusion(bf16[192,2048]{1,0:T(8,128)(2,1)S(1)} %fusion.15, s32[1024]{0:T(1024)S(1)} %pad_clamp_fusion.1), kind=kCustom, calls=%fused_computation | custom fusion | bytes 4720896 | tf_op jit(solution)/shard_map/gather | solution.py:107
  23.0 1.3 dynamic-slice_select_fusion
  24.3 22.1 %all_to_all.10 = bf16[4,144,512]{2,1,0:T(8,128)(2,1)} all-to-all(bf16[4,144,512]{2,1,0:T(8,128)(2,1)S(1)} %dynamic-slice_select_fusion), channel_id=1, replica_groups=mesh['grp'=2,'ep'=4,'tp'=4] {'ep'}, dimensions={0} | all-to-all | bytes 1179648 | tf_op jit(solution)/shard_map/all_to_all | solution.py:113
  46.5 23.3 %all-gather.5.cloned.1.call-done = bf16[4,144,2048]{2,1,0:T(8,128)(2,1)} async-done(((bf16[4,144,512]{2,1,0:T(8,128)(2,1)}), bf16[4,144,2048]{2,1,0:T(8,128)(2,1)}) %all-gather.5.cloned.1.call-update) | async-done | bytes 2359312 | tf_op jit(solution)/shard_map/all_gather | solution.py:112
  69.7 4.7 %fusion.9 = f32[576,512]{1,0:T(8,128)} fusion(bf16[576,2048]{1,0:T(8,128)(2,1)} %bitcast.131, bf16[1,2048,512]{2,1,0:T(8,128)(2,1)} %param.25), kind=kOutput, calls=%fused_computation.15 | convolution fusion | flops 1207959552 | bytes 5636096 | tf_op jit(solution)/shard_map/dot_general | solution.py:120
  74.5 6.7 %convolution_convert_fusion = bf16[576,2048]{1,0:T(8,128)(2,1)} fusion(bf16[1,512,2048]{2,1,0:T(8,128)(2,1)S(1)} %copy-done, bf16[576,2048]{1,0:T(8,128)(2,1)} %bitcast.132, bf16[1,2048,512]{2,1,0:T(8,128)(2,1)} %param.26, f32[576,512]{1,0:T(8,128)} %fusion.9), kind=kOutput, calls=%fused_computation.9 | convolution fusion | flops 2418868224 | bytes 10092544 | tf_op jit(solution)/shard_map/dot_general | solution.py:123
  81.3 0.8 copy-done.2
  83.8 0.8 constant_dynamic-slice_fusion
  85.3 13.9 %all_gather.12 = bf16[1024,128]{1,0:T(8,128)(2,1)S(1)} all-gather(bf16[256,128]{1,0:T(8,128)(2,1)S(1)} %get-tuple-element.2), channel_id=1, replica_groups=mesh['grp'=2,'ep'=4,'tp'=4] {'ep'}, dimensions={0}, use_global_device_ids=true | all-gather | bytes 327680 | tf_op jit(solution)/shard_map/all_gather | solution.py:72
  99.2 14.7 %all_gather.13 = bf16[1024,128]{0,1:T(8,128)(2,1)S(1)} all-gather(bf16[256,128]{0,1:T(8,128)(2,1)S(1)} %copy.34), channel_id=1, replica_groups=mesh['grp'=2,'ep'=4,'tp'=4] {'ep'}, dimensions={0}, use_global_device_ids=true | all-gather | bytes 327680 | tf_op jit(solution)/shard_map/all_gather | solution.py:73
  113.9 0.7 bitcast_reduce_fusion
  114.6 0.7 fusion.1
  115.4 1.6 %fusion.31 = bf16[1,128,256,4]{2,1,3,0:T(8,128)(2,1)} fusion(f32[1024,256,4]{1,0,2:T(8,128)S(1)} %get-tuple-element.14, f32[256,4]{0,1:T(4,128)S(1)} %get-tuple-element.13, bf16[1024,128]{0,1:T(8,128)(2,1)S(1)} %all_gather.13, f32[256,4]{0,1:T(4,128)S(1)} %get-tuple-element.10, f32[256,4]{0,1:T(4,128)S(1)} %get-tuple-element.9), kind=kOutput, calls=%fused_computation.30 | convolution fusion | flops 271974400 | bytes 4730880 | tf_op jit(solution)/shard_map/qkgn,nkd->qkgd/dot_general | solution.py:84
  117.0 4.8 %all-to-all-start.1 = ((bf16[4,144,512]{2,1,0:T(8,128)(2,1)}), bf16[4,144,512]{2,1,0:T(8,128)(2,1)S(1)}, u32[]{:S(2)}, u32[]{:S(2)}) async-start(bf16[4,144,512]{2,1,0:T(8,128)(2,1)} %reduce-scatter.2.cloned.1.call-done), calls=%async_computation.2 | async-start | bytes 1179648 | tf_op jit(solution)/shard_map/all_to_all | solution.py:130
  122.0 12.0 %all-gather.3.cloned.1.call-done = bf16[256,2048]{0,1:T(8,128)(2,1)} async-done(((bf16[256,512]{0,1:T(8,128)(2,1)}), bf16[256,2048]{0,1:T(8,128)(2,1)}) %all-gather.3.cloned.1.call-update) | async-done | bytes 1048592 | tf_op jit(solution)/shard_map/all_gather | solution.py:90
  134.0 3.3 %convolution_convert_fusion.1 = bf16[256,512]{1,0:T(8,128)(2,1)} fusion(bf16[256,2048]{0,1:T(8,128)(2,1)} %all-gather.3.cloned.1.call-done, bf16[2048,512]{1,0:T(8,128)(2,1)} %param.19), kind=kOutput, calls=%fused_computation.28 | convolution fusion | flops 537001984 | bytes 3407872 | tf_op jit(solution)/shard_map/dot_general | solution.py:89
  137.3 2.1 %gather_fusion.1 = bf16[384,512]{1,0:T(8,128)(2,1)S(1)} fusion(bf16[576,512]{1,0:T(8,128)(2,1)S(1)} %bitcast.122, s32[1024]{0:T(1024)S(1)} %pad_clamp_fusion), kind=kCustom, calls=%fused_computation.1 | custom fusion | bytes 787968 | tf_op jit(solution)/shard_map/gather | solution.py:132
  139.9 1.7 %multiply_reduce_fusion = bf16[192,512]{1,0:T(8,128)(2,1)} fusion(f32[192,2,512]{2,1,0:T(2,128)S(1)} %reshape.352, f32[192,2]{1,0:T(8,128)S(1)} %copy.28), kind=kLoop, calls=%fused_computation.31 | loop fusion | flops 294912 | bytes 984576 | tf_op jit(solution)/shard_map/reduce_sum | solution.py:134
  (68 shorter events, 4.9 us)
Async XLA Ops:
  7.2 67.3 %copy-start = (bf16[1,512,2048]{2,1,0:T(8,128)(2,1)S(1)}, bf16[1,512,2048]{2,1,0:T(8,128)(2,1)}, u32[]{:S(2)}) copy-start(bf16[1,512,2048]{2,1,0:T(8,128)(2,1)} %param.27) | copy-start | bytes 6291460
  7.2 62.6 %all-gather.5.cloned.1.call-start = ((), (), s32[]{:S(2)}) async-start(), calls=%async_computation.4 | async-start | bytes 2949120 | tf_op jit(solution)/shard_map/all_gather | solution.py:112
  46.4 70.6 %reduce-scatter.2.cloned.1.call-start = ((), (), s32[]{:S(2)}) async-start(), calls=%async_computation.5 | async-start | bytes 2949120 | tf_op jit(solution)/shard_map/reduce_scatter | solution.py:126
  81.2 0.9 copy-start.2
  81.2 1.1 copy-start.4
  81.2 2.4 %copy-start.1 = (bf16[256,512]{1,0:T(8,128)(2,1)S(1)}, bf16[256,512]{1,0:T(8,128)(2,1)}, u32[]{:S(2)}) copy-start(bf16[256,512]{1,0:T(8,128)(2,1)} %param.14) | copy-start | bytes 786436
  81.2 2.5 %copy-start.5 = (f32[128]{0:T(128)S(1)}, f32[128]{0:T(128)}, u32[]{:S(2)}) copy-start(f32[128]{0:T(128)} %param.17) | copy-start | bytes 1540
  81.2 52.8 %all-gather.3.cloned.1.call-start = ((), (), s32[]{:S(2)}) async-start(), calls=%async_computation.3 | async-start | bytes 1310720 | tf_op jit(solution)/shard_map/all_gather | solution.py:90
  115.3 6.4 %copy-start.3 = (f32[192,2]{0,1:T(2,128)S(1)}, f32[192,2]{0,1:T(2,128)}, u32[]{:S(2)}) copy-start(f32[192,2]{0,1:T(2,128)} %param.23) | copy-start | bytes 4612
  115.3 6.5 %copy-start.6 = (f32[192]{0:T(256)S(1)}, f32[192]{0:T(256)}, u32[]{:S(2)}) copy-start(f32[192]{0:T(256)} %param.22) | copy-start | bytes 2308
  117.0 20.3 %all-to-all-start.1 = ((bf16[4,144,512]{2,1,0:T(8,128)(2,1)}), bf16[4,144,512]{2,1,0:T(8,128)(2,1)S(1)}, u32[]{:S(2)}, u32[]{:S(2)}) async-start(bf16[4,144,512]{2,1,0:T(8,128)(2,1)} %reduce-scatter.2.cloned.1.call-done), calls=%async_computation.2 | async-start | bytes 1179648 | tf_op jit(solution)/shard_map/all_to_all | solution.py:130
Sparse Core Ops, SparseCore 0:
  46.5 23.1 all-gather.4
  81.3 32.7 reduce-scatter.1
  117.1 16.8 all-gather.2
where the time goes:
time: 149 us; the launch traced here: 148 us
  blocking collectives  50.8 us (34%)
  waiting for transfers between devices  35.3 us (24%)
  matrix products  17.1 us (11%)
  local copies, waits for them, and re-layouts  15.8 us (11%)
  between operations  14.1 us (9%)
  other arithmetic  10.1 us (7%)
  starting transfers between devices  4.88 us (3%)
    all_gather x1, waiting for transfers between devices, per_device(): lax.all_gather(lax.all_to_all(mine, 'ep', split_axis=0, concat_axis=0, ti...  23.3 us
    all_to_all x1, blocking collectives, per_device(): lax.all_to_all(mine, 'ep', split_axis=0, concat_axis=0, tiled=True)  22.1 us
    all_gather x1, blocking collectives, per_device(): v_piece = lax.all_gather(v_mine, 'ep', axis=0, tiled=True)  14.7 us
    all_gather x1, blocking collectives, per_device(): k_piece = lax.all_gather(k_rot, 'ep', axis=0, tiled=True)  13.9 us
    all_gather x1, waiting for transfers between devices, per_device(): lax.all_gather(mixed, 'tp', axis=1, tiled=True)  12 us
    dot_general x1, matrix products, per_device(): jnp.dot(hidden, w_down[0], preferred_element_type=jnp.float32)  6.71 us
    all_to_all x1, starting transfers between devices, per_device(): back = lax.all_to_all(summed, 'ep', split_axis=0, concat_axis=0, tiled=True)  4.76 us
    dot_general x1, matrix products, per_device(): gate = jnp.dot(flat, w_gate[0], preferred_element_type=jnp.float32)  4.74 us
  transfers between devices with their start and end apart: 4, of which 2 were waited for; matrix products, arithmetic and copies ran while one was open for 6% of the time, Pallas kernels for 0%

commit v1 on v0

v1 whole, which is shorter than its diff:
```python
import functools

import jax
import jax.numpy as jnp
import numpy as np
from jax import lax
from jax.experimental import pallas as pl
from jax.experimental.pallas import tpu as pltpu
from jax.sharding import PartitionSpec as P

HEADS = 16
KV_HEADS = 4
HEAD_DIM = 128
GRID_W = 64
TOPK = 2
CORES = 2
F32 = jnp.float32
BF16 = jnp.bfloat16
MESH = pl.DeviceIdType.MESH


def dot(a, b):
    return jnp.dot(a, b, preferred_element_type=F32)


def rope_tables(count):
    nfreq = HEAD_DIM // 4
    inverse = 10000.0 ** (-np.arange(nfreq, dtype=np.float32) / np.float32(nfreq))
    inverse = np.tile(inverse.astype(np.float32), 4)[None, :]
    sign = np.where(np.arange(HEAD_DIM) // nfreq % 2 == 0, -1.0, 1.0)[None, :]
    angle = np.arange(max(count, 8), dtype=np.float32)[:, None] * inverse
    wide = angle.astype(np.float64)
    return np.stack([np.cos(wide), np.sin(wide) * sign]).astype(np.float32)


def head_norm_rotate(x, gain, cosine, sine):
    wide = x.astype(F32)
    wide = wide * lax.rsqrt(jnp.mean(wide * wide, axis=-1, keepdims=True) + 1e-06) * gain
    n = HEAD_DIM // 4
    lane = lax.broadcasted_iota(jnp.int32, wide.shape, 1)
    turned = jnp.where(lane // n % 2 == 0, pltpu.roll(wide, HEAD_DIM - n, 1), pltpu.roll(wide, n, 1))
    return (wide * cosine + turned * sine).astype(BF16)


def kernel(
    E, T, C,
    q_ref, k_ref, v_ref, qg_ref, kg_ref, rowtab_ref, coltab_ref, rows_ref, routes_ref, routes_t_ref,
    gate_ref, logit_ref, mgain_ref, wo_hbm, wg_hbm, wu_hbm, wd_hbm,
    attn_ref, moe_ref,
    wo, wg, wu, wd, kvbuf, qrot, xn, dsend, xbuf, ysend, yown, yrecv, zsend, zrecv, fsend, back, obuf,
    cosb, sinb,
    w_sem, kv_s, kv_r, dp_s, dp_r, fw_s, fw_r, r1_s, r1_r, r2_s, r2_r, rt_s, rt_r, o_s, o_r, os_s, os_r,
):
    X = T // CORES
    ep, tp = lax.axis_index("ep"), lax.axis_index("tp")
    x, c = tp // CORES, tp % CORES
    sib = x * CORES + (1 - c)
    R, M, W = q_ref.shape[0], rows_ref.shape[0], rows_ref.shape[1]
    HW, F, HS, HO = W // 2, wg.shape[1], wd.shape[1] // T, q_ref.shape[1]
    heads_dev = HO // HEAD_DIM
    group = HEADS // KV_HEADS

    def peer_ep(d):
        return lax.rem(ep + (d + E) % E, E)

    def peer_x(d):
        return lax.rem(x + (d + X) % X, X) * CORES + c

    weights = [
        pltpu.make_async_copy(s, t, w_sem.at[i])
        for i, (s, t) in enumerate(((wg_hbm.at[0], wg), (wu_hbm.at[0], wu), (wd_hbm.at[0], wd), (wo_hbm, wo)))
    ]
    for w in weights:
        w.start()
    barrier = pltpu.get_barrier_semaphore()
    for d in range(1, E):
        pl.semaphore_signal(barrier, inc=1, device_id={"ep": peer_ep(d)}, device_id_type=MESH)
    for d in range(1, X):
        pl.semaphore_signal(barrier, inc=1, device_id={"tp": peer_x(d)}, device_id_type=MESH)
    pl.semaphore_signal(barrier, inc=1, device_id={"tp": sib}, device_id_type=MESH)

    sends = []

    def remote(src, dst, s, r, **where):
        return pltpu.make_async_remote_copy(
            src_ref=src, dst_ref=dst, send_sem=s, recv_sem=r, device_id=where, device_id_type=MESH
        )

    def send(*args, **where):
        copy = remote(*args, **where)
        copy.start()
        sends.append(copy)

    lane = lax.broadcasted_iota(jnp.int32, (GRID_W, HEAD_DIM), 1)
    for r in range(R // GRID_W):
        at = ep * (R // GRID_W) + r
        for i, buf in enumerate((cosb, sinb)):
            row = rowtab_ref[i, pl.ds(at, 1), :]
            buf[r * GRID_W : (r + 1) * GRID_W, :] = jnp.where(
                lane < HEAD_DIM // 2, jnp.broadcast_to(row, (GRID_W, HEAD_DIM)), coltab_ref[i, :GRID_W, :]
            )
    kv = pl.ds(pl.multiple_of(tp * heads_dev // group * HEAD_DIM, HEAD_DIM), HEAD_DIM)
    kvbuf[ep, 0] = head_norm_rotate(k_ref[:, kv], kg_ref[...], cosb[...], sinb[...])
    kvbuf[ep, 1] = v_ref[:, kv]

    wide = rows_ref[...].astype(F32)
    xn[...] = (
        wide * lax.rsqrt(jnp.mean(wide * wide, axis=-1, keepdims=True) + 1e-06) * mgain_ref[...]
    ).astype(BF16)

    def relative(v):
        return jnp.where(v >= ep, v - ep, v - ep + E)

    pad = -(-E // 16) * 16
    rt = relative(routes_t_ref[...])
    which = lax.broadcasted_iota(jnp.int32, (pad, M), 0)
    named = (which == rt[0:1, :]) | (which == rt[1:2, :])
    i0 = lax.broadcasted_iota(jnp.int32, (M, M), 0)
    i1 = lax.broadcasted_iota(jnp.int32, (M, M), 1)
    rank = dot(jnp.where(named, 1.0, 0.0).astype(BF16), jnp.where(i0 < i1, 1.0, 0.0).astype(BF16))
    rank = jnp.where(named, rank, -1.0)
    slot = lax.broadcasted_iota(jnp.int32, (C, M), 0).astype(F32)

    def picker(d):
        return jnp.where(slot == rank[d : d + 1, :], 1.0, 0.0).astype(BF16)

    pl.semaphore_wait(barrier, E - 1 + X - 1 + 1)
    for d in range(1, E):
        send(kvbuf.at[ep], kvbuf.at[ep], kv_s.at[d], kv_r.at[d], ep=peer_ep(d))
    half = pl.ds(pl.multiple_of(c * HW, 128), HW)
    for d in range(1, E):
        dsend[d] = dot(picker(d), xn[:, half]).astype(BF16)
        send(dsend.at[d], xbuf.at[d, c], dp_s.at[d], dp_r.at[d], ep=peer_ep(d))
    for h in range(2):
        xbuf[0, h] = dot(picker(0), xn[:, h * HW : (h + 1) * HW]).astype(BF16)

    for h in range(heads_dev):
        cols = slice(h * HEAD_DIM, (h + 1) * HEAD_DIM)
        qrot[:, cols] = head_norm_rotate(q_ref[:, cols], qg_ref[...], cosb[...], sinb[...])

    def arrive(d):
        remote(dsend.at[d], xbuf.at[d, c], dp_s.at[d], dp_r.at[d], ep=peer_ep(d)).wait_recv()
        send(xbuf.at[d, c], xbuf.at[d, c], fw_s.at[d], fw_r.at[d], tp=sib)

    def expert(d):
        if d:
            remote(xbuf.at[d, c], xbuf.at[d, 1 - c], fw_s.at[d], fw_r.at[d], tp=sib).wait_recv()
        x0, x1 = xbuf[d, 0], xbuf[d, 1]
        g = dot(x0, wg[:HW]) + dot(x1, wg[HW:])
        u = dot(x0, wu[:HW]) + dot(x1, wu[HW:])
        hidden = (g * jax.nn.sigmoid(g) * u).astype(BF16)
        for core, buf in ((1 - c, ysend), (c, yown)):
            for dx in range(X):
                t = lax.rem(x + dx, X) * CORES + core
                cols = pl.ds(pl.multiple_of(t * HS, HS), HS)
                buf[d, dx] = dot(hidden, wd[:, cols]).astype(BF16)
            if buf is ysend:
                send(ysend.at[d], yrecv.at[d], r1_s.at[d], r1_r.at[d], tp=sib)

    def pair(d):
        remote(ysend.at[d], yrecv.at[d], r1_s.at[d], r1_r.at[d], tp=sib).wait_recv()
        for dx in range(1, X):
            zsend[d, dx] = (yown[d, dx].astype(F32) + yrecv[d, dx].astype(F32)).astype(BF16)
            send(zsend.at[d, dx], zrecv.at[d, dx], r2_s.at[d, dx], r2_r.at[d, dx], tp=peer_x(dx))

    def total(d):
        value = yown[d, 0].astype(F32) + yrecv[d, 0].astype(F32)
        for dx in range(1, X):
            remote(
                zsend.at[d, dx], zrecv.at[d, dx], r2_s.at[d, dx], r2_r.at[d, dx], tp=peer_x(dx)
            ).wait_recv()
            value = value + zrecv[d, dx].astype(F32)
        if d == 0:
            back[0] = value.astype(BF16)
        else:
            fsend[d] = value.astype(BF16)
            send(fsend.at[d], back.at[d], rt_s.at[d], rt_r.at[d], ep=peer_ep(-d))

    for w in weights[:3]:
        w.wait()
    expert(0)

    for d in range(1, E):
        remote(kvbuf.at[ep], kvbuf.at[peer_ep(-d)], kv_s.at[d], kv_r.at[d], ep=peer_ep(d)).wait_recv()
    keys = kvbuf[:, 0].reshape(E * R, HEAD_DIM)
    vals = kvbuf[:, 1].reshape(E * R, HEAD_DIM)
    for h in range(heads_dev):
        cols = slice(h * HEAD_DIM, (h + 1) * HEAD_DIM)
        s = lax.dot_general(
            qrot[:, cols], keys, (((1,), (1,)), ((), ())), preferred_element_type=F32
        ) * HEAD_DIM ** (-0.5)
        e = jnp.exp(s - jnp.max(s, axis=-1, keepdims=True))
        l = jnp.sum(e, axis=-1, keepdims=True)
        obuf[tp, :, cols] = (dot(e.astype(BF16), vals) / l).astype(BF16)
    for dx in range(1, X):
        send(obuf.at[tp], obuf.at[tp], o_s.at[dx], o_r.at[dx], tp=peer_x(dx))
    send(obuf.at[tp], obuf.at[tp], os_s.at[0], os_r.at[0], tp=sib)

    def forward_heads():
        for dx in range(1, X):
            src = peer_x(-dx)
            remote(obuf.at[tp], obuf.at[src], o_s.at[dx], o_r.at[dx], tp=peer_x(dx)).wait_recv()
            send(obuf.at[src], obuf.at[src], os_s.at[dx], os_r.at[dx], tp=sib)

    def project():
        weights[3].wait()
        for dx in range(X):
            src = lax.rem(x + (X - dx) % X, X) * CORES + (1 - c)
            remote(obuf.at[tp], obuf.at[src], os_s.at[dx], os_r.at[dx], tp=sib).wait_recv()
        acc = dot(obuf[0], wo[:HO])
        for t in range(1, T):
            acc = acc + dot(obuf[t], wo[t * HO : (t + 1) * HO])
        attn_ref[...] = acc.astype(BF16)

    for d in range(1, E):
        arrive(d)
        pair(d - 1)
        expert(d)
        if d >= 2:
            total(d - 2)
    forward_heads()
    pair(E - 1)
    total(E - 2)
    project()
    total(E - 1)

    rm = relative(routes_ref[...])
    mwhich = lax.broadcasted_iota(jnp.int32, (M, 128), 1)
    first, second = mwhich == rm[:, 0:1], mwhich == rm[:, 1:2]
    mnamed = first | second
    mrank = dot(jnp.where(i1 < i0, 1.0, 0.0).astype(BF16), jnp.where(mnamed, 1.0, 0.0).astype(BF16))
    mrank = jnp.where(mnamed, mrank, -1.0)
    l0, l1 = logit_ref[:, 0:1], logit_ref[:, 1:2]
    top = jnp.maximum(l0, l1)
    e0, e1 = jnp.exp(l0 - top), jnp.exp(l1 - top)
    share0, share1 = gate_ref[...] * (e0 / (e0 + e1)), gate_ref[...] * (e1 / (e0 + e1))
    shares = jnp.where(first, share0, 0.0) + jnp.where(second, share1, 0.0)
    mslot = lax.broadcasted_iota(jnp.int32, (M, C), 1).astype(F32)
    out = jnp.zeros((M, HS), F32)
    for d in range(E):
        if d:
            remote(fsend.at[d], back.at[d], rt_s.at[d], rt_r.at[d], ep=peer_ep(-d)).wait_recv()
        pick = jnp.where(mslot == mrank[:, d : d + 1], 1.0, 0.0).astype(BF16)
        out = out + shares[:, d : d + 1] * dot(pick, back[d])
    moe_ref[...] = out.astype(BF16)
    for copy in sends:
        copy.wait_send()


def per_device(
    queries, keys, values, q_gain, k_gain, w_out, moe_rows, routes, group_gate, expert_logits, moe_gain,
    w_gate, w_up, w_down,
):
    E, T = lax.axis_size("ep"), lax.axis_size("tp")
    X = T // CORES
    R, HO = queries.shape
    M, W = moe_rows.shape
    F = w_gate.shape[2]
    HS = W // T
    C = -(-(3 * M // E) // 16) * 16
    vmem, hbm = pl.BlockSpec(memory_space=pltpu.VMEM), pl.BlockSpec(memory_space=pl.ANY)
    dma = lambda *shape: pltpu.SemaphoreType.DMA(shape)
    buf = lambda *shape: pltpu.VMEM(shape, BF16)
    return pl.pallas_call(
        functools.partial(kernel, E, T, C),
        out_shape=(jax.ShapeDtypeStruct((R, w_out.shape[1]), BF16), jax.ShapeDtypeStruct((M, HS), BF16)),
        in_specs=[vmem] * 13 + [hbm] * 4,
        out_specs=(vmem, vmem),
        scratch_shapes=[
            buf(*w_out.shape), buf(W, F), buf(W, F), buf(F, W),
            buf(E, 2, R, HEAD_DIM), buf(R, HO), buf(M, W), buf(E, C, W // 2), buf(E, 2, C, W // 2),
            buf(E, X, C, HS), buf(E, X, C, HS), buf(E, X, C, HS), buf(E, X, C, HS), buf(E, X, C, HS),
            buf(E, C, HS), buf(E, C, HS), buf(T, R, HO),
            pltpu.VMEM((R, HEAD_DIM), F32), pltpu.VMEM((R, HEAD_DIM), F32),
            dma(4), dma(E), dma(E), dma(E), dma(E), dma(E), dma(E), dma(E), dma(E),
            dma(E, X), dma(E, X), dma(E), dma(E), dma(X), dma(X), dma(X), dma(X),
        ],
        compiler_params=pltpu.CompilerParams(
            collective_id=0, has_side_effects=True, vmem_limit_bytes=56 * 1024 * 1024
        ),
        name="layer",
    )(
        queries, keys, values, q_gain[None], k_gain[None],
        jnp.asarray(rope_tables(R * E // GRID_W)), jnp.asarray(rope_tables(GRID_W)),
        moe_rows, routes, routes.T, group_gate[:, None], expert_logits, moe_gain[None],
        w_out, w_gate, w_up, w_down,
    )


def solution(mesh):
    placed = (
        P(("grp", "ep"), "tp"),
        P(("grp", "ep"), None),
        P(("grp", "ep"), None),
        P(),
        P(),
        P(None, "tp"),
        P(("grp", "ep"), None),
        P(("grp", "ep"), None),
        P(("grp", "ep")),
        P(("grp", "ep"), None),
        P(),
        P("ep", None, "tp"),
        P("ep", None, "tp"),
        P("ep", "tp", None),
    )
    return jax.shard_map(
        per_device,
        mesh=mesh,
        in_specs=placed,
        out_specs=(P(("grp", "ep"), "tp"), P(("grp", "ep"), "tp")),
        check_vma=False,
    )
```

time: 149 us -> 73.1 us (0.49)
  Pallas kernels: 0 us -> 64.6 us
  blocking collectives: 50.8 us -> 0 us
  waiting for transfers between devices: 35.3 us -> 0 us
  matrix products: 17.1 us -> 0 us
  between operations: 14.1 us -> 0.64 us
  other arithmetic: 10.1 us -> 0 us
  local copies, waits for them, and re-layouts: 15.8 us -> 7.62 us
  starting transfers between devices: 4.88 us -> 0 us
    pallas_call x0 -> x1, Pallas kernels: none -> 64.6 us  [per_device(): pl.pallas_call(functools.partial(kernel, E, T, C), out_shape=(jax.ShapeDt...]
    all_gather x2 -> x0, waiting for transfers between devices: 35.3 us -> none  [the longest x1 23.3 us: per_device(): lax.all_gather(lax.all_to_all(mine, 'ep', split_axis=0, concat_axis=0, ti...]
    all_gather x2 -> x0, blocking collectives: 28.6 us -> none  [the longest x1 14.7 us: per_device(): v_piece = lax.all_gather(v_mine, 'ep', axis=0, tiled=True)]
    all_to_all x1 -> x0, blocking collectives: 22.1 us -> none  [per_device(): lax.all_to_all(mine, 'ep', split_axis=0, concat_axis=0, tiled=True)]
    dot_general x5 -> x0, matrix products: 17.1 us -> none  [the longest x1 6.71 us: per_device(): jnp.dot(hidden, w_down[0], preferred_element_type=jnp.float32)]
    gather x2 -> x0, local copies, waits for them, and re-layouts: 6.07 us -> none  [the longest x1 4.01 us: per_device(): normed[source]]
    scatter x2 -> x0, local copies, waits for them, and re-layouts: 4.89 us -> none  [the longest x1 2.92 us: per_device(): source = jnp.zeros((peers * capacity,), jnp.int32).at[slots].set(owner)]
    all_to_all x1 -> x0, starting transfers between devices: 4.76 us -> none  [per_device(): back = lax.all_to_all(summed, 'ep', split_axis=0, concat_axis=0, tiled=True)]
  transfers between devices with their start and end apart: 4 -> 0, of which waited for: 2 -> 0; matrix products, arithmetic and copies ran while one was open for 6% -> 0% of each run, Pallas kernels for 0% -> 0%
where the time goes in v1:
time: 73.1 us; the launch traced here: 72.8 us
  Pallas kernels  64.6 us (88%)
  local copies, waits for them, and re-layouts  7.62 us (10%)
    pallas_call x1, Pallas kernels, per_device(): pl.pallas_call(functools.partial(kernel, E, T, C), out_shape=(jax.ShapeDt...  64.6 us
    unnamed x4, local copies, waits for them, and re-layouts  6.18 us

profile of v1, /device:TPU:0, one launch (start us, length us, event | category | flops | bytes accessed | tf_op | source)
XLA Modules:
  0.0 72.8 jit_solution(14206920726026609558)
XLA Ops:
  0.6 1.4 %copy.21.gate_ref = f32[192,1]{1,0:T(8,128)} copy(f32[192,1]{0,1:T(1,128)} %bitcast.7) | data formatting | bytes 1536 | tf_op jit(solution)/shard_map/broadcast_in_dim | solution.py:285
  2.1 1.4 %copy.22.logit_ref = f32[192,2]{1,0:T(8,128)} copy(f32[192,2]{0,1:T(2,128)} %param.25) | data formatting | bytes 3072 | tf_op args[9]
  3.5 1.4 %copy.20.routes_ref = s32[192,2]{1,0:T(8,128)} copy(s32[192,2]{0,1:T(2,128)} %param.23) | data formatting | bytes 3072 | tf_op args[7]
  5.0 64.6 %layer.1 = (bf16[256,512]{1,0:T(8,128)(2,1)}, bf16[192,512]{1,0:T(8,128)(2,1)}) custom-call(bf16[256,512]{1,0:T(8,128)(2,1)} %q_ref.1, bf16[256,512]{1,0:T(8,128)(2,1)} %k_ref.1, bf16[256,512]{1,0:T(8,128)(2,1)} %v_ref.1, f32[1,128]{1,0:T(1,128)} %bitcast.8, f32[1,128]{1,0:T(1,128)} %bitcast.9, f32[2,16,128]{2,1,0:T(8,128)} %constant.4.clone.rowtab_ref, ...), custom_call_target="tpu_custom_call" | custom-call | tf_op jit(solution)/shard_map/layer/pallas_call | solution.py:264
  69.6 1.7 %copy.25 = bf16[256,512]{1,0:T(8,128)(2,1)} copy(bf16[256,512]{1,0:T(8,128)(2,1)} %get-tuple-element.4) | data formatting | bytes 524288
  71.2 1.6 %copy.26 = bf16[192,512]{1,0:T(8,128)(2,1)} copy(bf16[192,512]{1,0:T(8,128)(2,1)} %get-tuple-element.5) | data formatting | bytes 393216

commit v2 on v1

--- a/solution.py
+++ b/solution.py
@@ -44,19 +44,19 @@
 
 def kernel(
     E, T, C,
-    q_ref, k_ref, v_ref, qg_ref, kg_ref, rowtab_ref, coltab_ref, rows_ref, routes_ref, routes_t_ref,
+    q_ref, k_ref, v_ref, qg_ref, kg_ref, rowtab_ref, coltab_ref, rows_ref, routes_ref,
     gate_ref, logit_ref, mgain_ref, wo_hbm, wg_hbm, wu_hbm, wd_hbm,
     attn_ref, moe_ref,
     wo, wg, wu, wd, kvbuf, qrot, xn, dsend, xbuf, ysend, yown, yrecv, zsend, zrecv, fsend, back, obuf,
     cosb, sinb,
-    w_sem, kv_s, kv_r, dp_s, dp_r, fw_s, fw_r, r1_s, r1_r, r2_s, r2_r, rt_s, rt_r, o_s, o_r, os_s, os_r,
+    w_sem, kv_s, kv_r, dp_s, dp_r, dx_s, dx_r, fw_s, fw_r, r1_s, r1_r, r2_s, r2_r, rt_s, rt_r, o_s, o_r, os_s, os_r,
 ):
     X = T // CORES
     ep, tp = lax.axis_index("ep"), lax.axis_index("tp")
     x, c = tp // CORES, tp % CORES
     sib = x * CORES + (1 - c)
     R, M, W = q_ref.shape[0], rows_ref.shape[0], rows_ref.shape[1]
-    HW, F, HS, HO = W // 2, wg.shape[1], wd.shape[1] // T, q_ref.shape[1]
+    F, HS, HO = wg.shape[1], wd.shape[1] // T, q_ref.shape[1]
     heads_dev = HO // HEAD_DIM
     group = HEADS // KV_HEADS
 
@@ -91,6 +91,35 @@
         copy.start()
         sends.append(copy)
 
+    wide = rows_ref[...].astype(F32)
+    xn[...] = (
+        wide * lax.rsqrt(jnp.mean(wide * wide, axis=-1, keepdims=True) + 1e-06) * mgain_ref[...]
+    ).astype(BF16)
+
+    def relative(v):
+        return jnp.where(v >= ep, v - ep, v - ep + E)
+
+    pad = -(-E // 16) * 16
+    rt = relative(routes_ref[...])
+    which = lax.broadcasted_iota(jnp.int32, (pad, M), 0)
+    first, second = which == rt[0:1, :], which == rt[1:2, :]
+    named = first | second
+    i0 = lax.broadcasted_iota(jnp.int32, (M, M), 0)
+    i1 = lax.broadcasted_iota(jnp.int32, (M, M), 1)
+    rank = dot(jnp.where(named, 1.0, 0.0).astype(BF16), jnp.where(i0 < i1, 1.0, 0.0).astype(BF16))
+    rank = jnp.where(named, rank, -1.0)
+    slot = lax.broadcasted_iota(jnp.int32, (C, M), 0).astype(F32)
+
+    def picker(d):
+        return jnp.where(slot == rank[d : d + 1, :], 1.0, 0.0).astype(BF16)
+
+    mine = pl.ds(pl.multiple_of(tp * HS, 128), HS)
+    for d in range(1, E):
+        dsend[d] = dot(picker(d), xn[:, mine]).astype(BF16)
+        if d == 1:
+            pl.semaphore_wait(barrier, E - 1 + X - 1 + 1)
+        send(dsend.at[d], xbuf.at[d, tp], dp_s.at[d], dp_r.at[d], ep=peer_ep(d))
+
     lane = lax.broadcasted_iota(jnp.int32, (GRID_W, HEAD_DIM), 1)
     for r in range(R // GRID_W):
         at = ep * (R // GRID_W) + r
@@ -103,51 +132,35 @@
     kvbuf[ep, 0] = head_norm_rotate(k_ref[:, kv], kg_ref[...], cosb[...], sinb[...])
     kvbuf[ep, 1] = v_ref[:, kv]
 
-    wide = rows_ref[...].astype(F32)
-    xn[...] = (
-        wide * lax.rsqrt(jnp.mean(wide * wide, axis=-1, keepdims=True) + 1e-06) * mgain_ref[...]
-    ).astype(BF16)
-
-    def relative(v):
-        return jnp.where(v >= ep, v - ep, v - ep + E)
-
-    pad = -(-E // 16) * 16
-    rt = relative(routes_t_ref[...])
-    which = lax.broadcasted_iota(jnp.int32, (pad, M), 0)
-    named = (which == rt[0:1, :]) | (which == rt[1:2, :])
-    i0 = lax.broadcasted_iota(jnp.int32, (M, M), 0)
-    i1 = lax.broadcasted_iota(jnp.int32, (M, M), 1)
-    rank = dot(jnp.where(named, 1.0, 0.0).astype(BF16), jnp.where(i0 < i1, 1.0, 0.0).astype(BF16))
-    rank = jnp.where(named, rank, -1.0)
-    slot = lax.broadcasted_iota(jnp.int32, (C, M), 0).astype(F32)
-
-    def picker(d):
-        return jnp.where(slot == rank[d : d + 1, :], 1.0, 0.0).astype(BF16)
-
-    pl.semaphore_wait(barrier, E - 1 + X - 1 + 1)
     for d in range(1, E):
         send(kvbuf.at[ep], kvbuf.at[ep], kv_s.at[d], kv_r.at[d], ep=peer_ep(d))
-    half = pl.ds(pl.multiple_of(c * HW, 128), HW)
-    for d in range(1, E):
-        dsend[d] = dot(picker(d), xn[:, half]).astype(BF16)
-        send(dsend.at[d], xbuf.at[d, c], dp_s.at[d], dp_r.at[d], ep=peer_ep(d))
-    for h in range(2):
-        xbuf[0, h] = dot(picker(0), xn[:, h * HW : (h + 1) * HW]).astype(BF16)
+    for t in range(T):
+        xbuf[0, t] = dot(picker(0), xn[:, t * HS : (t + 1) * HS]).astype(BF16)
 
     for h in range(heads_dev):
         cols = slice(h * HEAD_DIM, (h + 1) * HEAD_DIM)
         qrot[:, cols] = head_norm_rotate(q_ref[:, cols], qg_ref[...], cosb[...], sinb[...])
 
     def arrive(d):
-        remote(dsend.at[d], xbuf.at[d, c], dp_s.at[d], dp_r.at[d], ep=peer_ep(d)).wait_recv()
-        send(xbuf.at[d, c], xbuf.at[d, c], fw_s.at[d], fw_r.at[d], tp=sib)
+        own = xbuf.at[d, tp]
+        remote(dsend.at[d], own, dp_s.at[d], dp_r.at[d], ep=peer_ep(d)).wait_recv()
+        for dx in range(1, X):
+            send(own, own, dx_s.at[d, dx], dx_r.at[d, dx], tp=peer_x(dx))
+        send(own, own, fw_s.at[d, 0], fw_r.at[d, 0], tp=sib)
+
+    def relay(d):
+        for dx in range(1, X):
+            theirs = xbuf.at[d, peer_x(-dx)]
+            remote(xbuf.at[d, tp], theirs, dx_s.at[d, dx], dx_r.at[d, dx], tp=peer_x(dx)).wait_recv()
+            send(theirs, theirs, fw_s.at[d, dx], fw_r.at[d, dx], tp=sib)
 
     def expert(d):
         if d:
-            remote(xbuf.at[d, c], xbuf.at[d, 1 - c], fw_s.at[d], fw_r.at[d], tp=sib).wait_recv()
-        x0, x1 = xbuf[d, 0], xbuf[d, 1]
-        g = dot(x0, wg[:HW]) + dot(x1, wg[HW:])
-        u = dot(x0, wu[:HW]) + dot(x1, wu[HW:])
+            for dx in range(X):
+                theirs = xbuf.at[d, lax.rem(x + (X - dx) % X, X) * CORES + (1 - c)]
+                remote(xbuf.at[d, tp], theirs, fw_s.at[d, dx], fw_r.at[d, dx], tp=sib).wait_recv()
+        rows = jnp.concatenate([xbuf[d, t] for t in range(T)], axis=1)
+        g, u = dot(rows, wg[...]), dot(rows, wu[...])
         hidden = (g * jax.nn.sigmoid(g) * u).astype(BF16)
         for core, buf in ((1 - c, ysend), (c, yown)):
             for dx in range(X):
@@ -176,26 +189,6 @@
             fsend[d] = value.astype(BF16)
             send(fsend.at[d], back.at[d], rt_s.at[d], rt_r.at[d], ep=peer_ep(-d))
 
-    for w in weights[:3]:
-        w.wait()
-    expert(0)
-
-    for d in range(1, E):
-        remote(kvbuf.at[ep], kvbuf.at[peer_ep(-d)], kv_s.at[d], kv_r.at[d], ep=peer_ep(d)).wait_recv()
-    keys = kvbuf[:, 0].reshape(E * R, HEAD_DIM)
-    vals = kvbuf[:, 1].reshape(E * R, HEAD_DIM)
-    for h in range(heads_dev):
-        cols = slice(h * HEAD_DIM, (h + 1) * HEAD_DIM)
-        s = lax.dot_general(
-            qrot[:, cols], keys, (((1,), (1,)), ((), ())), preferred_element_type=F32
-        ) * HEAD_DIM ** (-0.5)
-        e = jnp.exp(s - jnp.max(s, axis=-1, keepdims=True))
-        l = jnp.sum(e, axis=-1, keepdims=True)
-        obuf[tp, :, cols] = (dot(e.astype(BF16), vals) / l).astype(BF16)
-    for dx in range(1, X):
-        send(obuf.at[tp], obuf.at[tp], o_s.at[dx], o_r.at[dx], tp=peer_x(dx))
-    send(obuf.at[tp], obuf.at[tp], os_s.at[0], os_r.at[0], tp=sib)
-
     def forward_heads():
         for dx in range(1, X):
             src = peer_x(-dx)
@@ -212,29 +205,46 @@
             acc = acc + dot(obuf[t], wo[t * HO : (t + 1) * HO])
         attn_ref[...] = acc.astype(BF16)
 
+    def attend():
+        for d in range(1, E):
+            remote(kvbuf.at[ep], kvbuf.at[peer_ep(-d)], kv_s.at[d], kv_r.at[d], ep=peer_ep(d)).wait_recv()
+        keys = kvbuf[:, 0].reshape(E * R, HEAD_DIM)
+        vals = kvbuf[:, 1].reshape(E * R, HEAD_DIM)
+        for h in range(heads_dev):
+            cols = slice(h * HEAD_DIM, (h + 1) * HEAD_DIM)
+            s = lax.dot_general(
+                qrot[:, cols], keys, (((1,), (1,)), ((), ())), preferred_element_type=F32
+            ) * HEAD_DIM ** (-0.5)
+            e = jnp.exp(s - jnp.max(s, axis=-1, keepdims=True))
+            l = jnp.sum(e, axis=-1, keepdims=True)
+            obuf[tp, :, cols] = (dot(e.astype(BF16), vals) / l).astype(BF16)
+        for dx in range(1, X):
+            send(obuf.at[tp], obuf.at[tp], o_s.at[dx], o_r.at[dx], tp=peer_x(dx))
+        send(obuf.at[tp], obuf.at[tp], os_s.at[0], os_r.at[0], tp=sib)
+
+    for w in weights[:3]:
+        w.wait()
+    expert(0)
+    arrive(1)
+    pair(0)
     for d in range(1, E):
-        arrive(d)
-        pair(d - 1)
+        relay(d)
+        if d + 1 < E:
+            arrive(d + 1)
         expert(d)
-        if d >= 2:
-            total(d - 2)
+        total(d - 1)
+        pair(d)
+    attend()
+    total(E - 1)
     forward_heads()
-    pair(E - 1)
-    total(E - 2)
     project()
-    total(E - 1)
-
-    rm = relative(routes_ref[...])
-    mwhich = lax.broadcasted_iota(jnp.int32, (M, 128), 1)
-    first, second = mwhich == rm[:, 0:1], mwhich == rm[:, 1:2]
-    mnamed = first | second
-    mrank = dot(jnp.where(i1 < i0, 1.0, 0.0).astype(BF16), jnp.where(mnamed, 1.0, 0.0).astype(BF16))
-    mrank = jnp.where(mnamed, mrank, -1.0)
-    l0, l1 = logit_ref[:, 0:1], logit_ref[:, 1:2]
+
+    l0, l1 = logit_ref[0:1, :], logit_ref[1:2, :]
     top = jnp.maximum(l0, l1)
     e0, e1 = jnp.exp(l0 - top), jnp.exp(l1 - top)
     share0, share1 = gate_ref[...] * (e0 / (e0 + e1)), gate_ref[...] * (e1 / (e0 + e1))
-    shares = jnp.where(first, share0, 0.0) + jnp.where(second, share1, 0.0)
+    shares = (jnp.where(first, share0, 0.0) + jnp.where(second, share1, 0.0)).T
+    mrank = rank.T
     mslot = lax.broadcasted_iota(jnp.int32, (M, C), 1).astype(F32)
     out = jnp.zeros((M, HS), F32)
     for d in range(E):
@@ -245,6 +255,11 @@
     moe_ref[...] = out.astype(BF16)
     for copy in sends:
         copy.wait_send()
+
+
+def hand_over(a_ref, b_ref, attn_ref, moe_ref):
+    attn_ref[...] = a_ref[...]
+    moe_ref[...] = b_ref[...]
 
 
 def per_device(
@@ -261,18 +276,18 @@
     vmem, hbm = pl.BlockSpec(memory_space=pltpu.VMEM), pl.BlockSpec(memory_space=pl.ANY)
     dma = lambda *shape: pltpu.SemaphoreType.DMA(shape)
     buf = lambda *shape: pltpu.VMEM(shape, BF16)
-    return pl.pallas_call(
+    outs = pl.pallas_call(
         functools.partial(kernel, E, T, C),
         out_shape=(jax.ShapeDtypeStruct((R, w_out.shape[1]), BF16), jax.ShapeDtypeStruct((M, HS), BF16)),
-        in_specs=[vmem] * 13 + [hbm] * 4,
+        in_specs=[vmem] * 12 + [hbm] * 4,
         out_specs=(vmem, vmem),
         scratch_shapes=[
             buf(*w_out.shape), buf(W, F), buf(W, F), buf(F, W),
-            buf(E, 2, R, HEAD_DIM), buf(R, HO), buf(M, W), buf(E, C, W // 2), buf(E, 2, C, W // 2),
+            buf(E, 2, R, HEAD_DIM), buf(R, HO), buf(M, W), buf(E, C, HS), buf(E, T, C, HS),
             buf(E, X, C, HS), buf(E, X, C, HS), buf(E, X, C, HS), buf(E, X, C, HS), buf(E, X, C, HS),
             buf(E, C, HS), buf(E, C, HS), buf(T, R, HO),
             pltpu.VMEM((R, HEAD_DIM), F32), pltpu.VMEM((R, HEAD_DIM), F32),
-            dma(4), dma(E), dma(E), dma(E), dma(E), dma(E), dma(E), dma(E), dma(E),
+            dma(4), dma(E), dma(E), dma(E), dma(E), dma(E, X), dma(E, X), dma(E, X), dma(E, X), dma(E), dma(E),
             dma(E, X), dma(E, X), dma(E), dma(E), dma(X), dma(X), dma(X), dma(X),
         ],
         compiler_params=pltpu.CompilerParams(
@@ -282,9 +297,13 @@
     )(
         queries, keys, values, q_gain[None], k_gain[None],
         jnp.asarray(rope_tables(R * E // GRID_W)), jnp.asarray(rope_tables(GRID_W)),
-        moe_rows, routes, routes.T, group_gate[:, None], expert_logits, moe_gain[None],
+        moe_rows, routes.T, group_gate[None], expert_logits.T, moe_gain[None],
         w_out, w_gate, w_up, w_down,
     )
+    return pl.pallas_call(
+        hand_over, out_shape=tuple(jax.ShapeDtypeStruct(o.shape, BF16) for o in outs),
+        in_specs=[vmem] * 2, out_specs=(vmem, vmem), name="hand_over",
+    )(*outs)
 
 
 def solution(mesh):

time: 73.1 us -> 56.5 us (0.77)
  Pallas kernels: 64.6 us -> 55.7 us
  local copies, waits for them, and re-layouts: 7.62 us -> 0 us
    pallas_call x1, Pallas kernels: 64.6 us -> 54 us  [per_device(): pl.pallas_call(functools.partial(kernel, E, T, C), out_shape=(jax.ShapeDt...]
    unnamed x4 -> x0, local copies, waits for them, and re-layouts: 6.18 us -> none
    pallas_call x0 -> x1, Pallas kernels: none -> 1.79 us  [per_device(): pl.pallas_call(hand_over, out_shape=tuple((jax.ShapeDtypeStruct(o.shape,...]
    broadcast_in_dim x1 -> x0, local copies, waits for them, and re-layouts: 1.44 us -> none  [per_device(): group_gate[:, None]]
where the time goes in v2:
time: 56.5 us; the launch traced here: 56.4 us
  Pallas kernels  55.7 us (99%)
  between operations  0.64 us (1%)
    pallas_call x1, Pallas kernels, per_device(): pl.pallas_call(functools.partial(kernel, E, T, C), out_shape=(jax.ShapeDt...  54 us
    pallas_call x1, Pallas kernels, per_device(): pl.pallas_call(hand_over, out_shape=tuple((jax.ShapeDtypeStruct(o.shape,...  1.79 us

profile of v2, /device:TPU:0, one launch (start us, length us, event | category | flops | bytes accessed | tf_op | source)
XLA Modules:
  0.0 56.4 jit_solution(16182029031236366609)
XLA Ops:
  0.6 54.0 %layer.1 = (bf16[256,512]{1,0:T(8,128)(2,1)}, bf16[192,512]{1,0:T(8,128)(2,1)}) custom-call(bf16[256,512]{1,0:T(8,128)(2,1)} %q_ref.1, bf16[256,512]{1,0:T(8,128)(2,1)} %k_ref.1, bf16[256,512]{1,0:T(8,128)(2,1)} %v_ref.1, f32[1,128]{1,0:T(1,128)} %bitcast.10, f32[1,128]{1,0:T(1,128)} %bitcast.11, f32[2,16,128]{2,1,0:T(8,128)} %constant.4.clone.rowtab_ref, ...), custom_call_target="tpu_custom_call" | custom-call | tf_op jit(solution)/shard_map/layer/pallas_call | solution.py:279
  54.6 1.8 %hand_over.1 = (bf16[256,512]{1,0:T(8,128)(2,1)}, bf16[192,512]{1,0:T(8,128)(2,1)}) custom-call(bf16[256,512]{1,0:T(8,128)(2,1)} %get-tuple-element.4.a_ref, bf16[192,512]{1,0:T(8,128)(2,1)} %get-tuple-element.5.b_ref), custom_call_target="tpu_custom_call" | custom-call | tf_op jit(solution)/shard_map/hand_over/pallas_call | solution.py:303
